TPU v7x, 32 devices: a whole 2x2x4 slice. The times are simulated.
32 devices in a mesh: sp: 4 (over y, x), tp: 8 (over z, core).
Axes of the slice: x: 2, y: 2, z: 4, core: 2. Of those that a mesh axis runs over, the one named last changes fastest.
Arguments:
- resid: bfloat16 [2048, 2048], P(('sp', 'tp')), may hold values from -6 to 6
- query_a: bfloat16 [2048, 16, 128], P('sp', 'tp'), may hold values from -16 to 16
- key_a: bfloat16 [2048, 16, 128], P('sp', 'tp'), may hold values from -16 to 16
- value_a: bfloat16 [2048, 16, 128], P('sp', 'tp'), may hold values from -6 to 6
- query_b: bfloat16 [2048, 16, 64], P('sp', 'tp'), may hold values from -16 to 16
- key_b: bfloat16 [2048, 16, 64], P('sp', 'tp'), may hold values from -16 to 16
- value_b: bfloat16 [2048, 16, 64], P('sp', 'tp'), may hold values from -6 to 6
- mix_a: float32 [16], P('tp'), may hold values from 0.3 to 0.8
- mix_b: float32 [16], P('tp'), may hold values from 0.3 to 0.8
- head_gain_a: float32 [128], replicated, may hold values from 0.1 to 1.9
- head_gain_b: float32 [64], replicated, may hold values from 0.1 to 1.9
- proj_a: bfloat16 [2048, 2048], P('tp'), may hold values from -0.109375 to 0.109375
- proj_b: bfloat16 [1024, 2048], P('tp'), may hold values from -0.109375 to 0.109375
- norm_gain: float32 [2048], replicated, may hold values from 0.1 to 1.9
- route_ids: int32 [2048, 2], P(('sp', 'tp')), may hold values from 0 to 3, all different within a row; in each aligned block of 64 rows (0 to 63, 64 to 127, ...) at most 48 rows name the same one
- route_weights: float32 [2048, 2], P(('sp', 'tp')), may hold values from 0.2 to 1
- expert_gate: bfloat16 [4, 2048, 6144], P('sp', None, 'tp'), may hold values from -0.125 to 0.125
- expert_up: bfloat16 [4, 2048, 6144], P('sp', None, 'tp'), may hold values from -0.125 to 0.125
- expert_down: bfloat16 [4, 6144, 2048], P('sp', 'tp'), may hold values from -0.078125 to 0.078125
Outputs:
- out: bfloat16 [2048, 2048], P(('sp', 'tp'))
Inputs may be any that keep to these rules, and one draw needn't show every extreme that they name: `route_ids`: each row names 2 different experts. Within the rows of one device (aligned blocks of 64 rows) no expert is named by more than 48 rows, and in every draw some device's block names some expert exactly 48 times.
All inputs are finite; a program needn't handle non-finite values.
Results may differ from a plain program's by a relative error of at most 0.02.
Values may be sent and summed in bfloat16 or wider, within the bound.
No kernel may reach another device: no remote copies, remote signals or barrier semaphores. Data moves between devices by JAX's collectives and lax.ppermute only.
A program may use at most 128 MiB of HBM per device.

v0:
```python
import math
import jax
import jax.numpy as jnp
from jax import lax
from jax.sharding import PartitionSpec as P

EPS = 1e-06
NEG = -1e30
HEAD_SCALE = 1.0 - (0.8 - 0.6 * math.exp(-0.3))
KEY_STEP = 512


def partner(value, axis, apart):
    return lax.ppermute(value, axis, [(i, i ^ 1 << apart) for i in range(lax.axis_size(axis))])


def rms_scaled(values, gain):
    return values * lax.rsqrt(jnp.mean(values * values, axis=-1, keepdims=True) + EPS) * gain


def slot_numbers(route_rows, experts, capacity):
    count, top_count = route_rows.shape
    flat = route_rows.reshape(count * top_count)
    onehot = (flat[:, None] == jnp.arange(experts, dtype=jnp.int32)[None, :]).astype(jnp.int32)
    ranks = jnp.sum((jnp.cumsum(onehot, axis=0) - onehot) * onehot, axis=1)
    return (flat * capacity + ranks).reshape(count, top_count)


def empty_map(count, heads, width):
    return (
        jnp.zeros((count, heads, width), jnp.float32),
        jnp.full((heads, count), NEG, jnp.float32),
        jnp.zeros((heads, count), jnp.float32),
    )


def empty_group(query, value):
    return (
        empty_map(query.shape[0], query.shape[1], value.shape[2]),
        empty_map(query.shape[0], query.shape[1], value.shape[2]),
    )


def map_update(state, query, keys, values, allowed, scale):
    weighted, maximum, sums = state
    scores = jnp.einsum("qhd,khd->hqk", query, keys, preferred_element_type=jnp.float32) * scale
    scores = jnp.where(allowed[None], scores, NEG)
    fresh = jnp.maximum(maximum, jnp.max(scores, axis=2))
    weights = jnp.where(allowed[None], jnp.exp(scores - fresh[:, :, None]), 0.0)
    factor = jnp.exp(maximum - fresh)
    sums = sums * factor + jnp.sum(weights, axis=2)
    added = jnp.einsum(
        "hqk,khv->qhv", weights.astype(jnp.bfloat16), values, preferred_element_type=jnp.float32
    )
    weighted = weighted * jnp.transpose(factor)[:, :, None] + added
    return (weighted, fresh, sums)


def group_update(states, query, keys, values, allowed):
    width = query.shape[2] // 2
    scale = 1.0 / math.sqrt(width)
    return tuple(
        (
            map_update(
                states[which],
                query[:, :, which * width : (which + 1) * width],
                keys[:, :, which * width : (which + 1) * width],
                values,
                allowed,
                scale,
            )
            for which in range(2)
        )
    )


def set_update(carry, queries, pieces):
    rows_a, rows_b, query_pos = queries
    piece_key_a, piece_value_a, piece_key_b, piece_value_b = pieces
    length = piece_key_a.shape[0]
    step = math.gcd(length, KEY_STEP)
    latest = query_pos[-1]

    def inner(index, states):
        first = index * step

        def compute(current):
            keys_a = lax.dynamic_slice_in_dim(piece_key_a, first, step, 0)
            values_a = lax.dynamic_slice_in_dim(piece_value_a, first, step, 0)
            keys_b = lax.dynamic_slice_in_dim(piece_key_b, first, step, 0)
            values_b = lax.dynamic_slice_in_dim(piece_value_b, first, step, 0)
            key_pos = first + jnp.arange(step, dtype=jnp.int32)
            allowed = key_pos[None, :] <= query_pos[:, None]
            return (
                group_update(current[0], rows_a, keys_a, values_a, allowed),
                group_update(current[1], rows_b, keys_b, values_b, allowed),
            )

        return lax.cond(first <= latest, compute, lambda current: current, states)

    return lax.fori_loop(0, length // step, inner, carry)


def finish_group(states, mix, gain):
    outputs = [state[0] / jnp.transpose(state[2])[:, :, None] for state in states]
    mixed = outputs[0] - mix[None, :, None] * outputs[1]
    normed = rms_scaled(mixed, gain) * HEAD_SCALE
    return normed.astype(jnp.bfloat16).reshape(mixed.shape[0], -1)


def per_device(
    resid,
    query_a,
    key_a,
    value_a,
    query_b,
    key_b,
    value_b,
    mix_a,
    mix_b,
    head_gain_a,
    head_gain_b,
    proj_a,
    proj_b,
    norm_gain,
    route_ids,
    route_weights,
    expert_gate,
    expert_up,
    expert_down,
):
    seq_rows = query_a.shape[0]
    sp_ways = lax.axis_size("sp")
    place = lax.axis_index("sp")
    positions = place * seq_rows + jnp.arange(seq_rows, dtype=jnp.int32)
    levels = sp_ways.bit_length() - 1
    half = seq_rows // 2
    moved = jnp.concatenate(
        [query_a[half:].reshape(half, -1), query_b[half:].reshape(half, -1)], axis=1
    )
    for bit in range(levels):
        moved = partner(moved, "sp", bit)
    split_at = query_a.shape[1] * query_a.shape[2]
    far_a = moved[:, :split_at].reshape(half, query_a.shape[1], query_a.shape[2])
    far_b = moved[:, split_at:].reshape(half, query_b.shape[1], query_b.shape[2])
    far_pos = (sp_ways - 1 - place) * seq_rows + half + jnp.arange(half, dtype=jnp.int32)
    query_sets = ((query_a[:half], query_b[:half], positions[:half]), (far_a, far_b, far_pos))

    def fold_keys(carry, pieces):
        return tuple(
            (set_update(states, queries, pieces) for states, queries in zip(carry, query_sets))
        )

    initial = tuple(
        (
            (empty_group(queries[0], value_a), empty_group(queries[1], value_b))
            for queries in query_sets
        )
    )
    results = fold_keys(
        initial,
        (
            lax.all_gather(key_a, "sp", axis=0, tiled=True),
            lax.all_gather(value_a, "sp", axis=0, tiled=True),
            lax.all_gather(key_b, "sp", axis=0, tiled=True),
            lax.all_gather(value_b, "sp", axis=0, tiled=True),
        ),
    )
    finished = [
        (finish_group(states[0], mix_a, head_gain_a), finish_group(states[1], mix_b, head_gain_b))
        for states in results
    ]
    returned = jnp.concatenate([finished[1][0], finished[1][1]], axis=1)
    for bit in range(levels):
        returned = partner(returned, "sp", bit)
    width_a = finished[0][0].shape[1]
    heads_out_a = jnp.concatenate([finished[0][0], returned[:, :width_a]], axis=0)
    heads_out_b = jnp.concatenate([finished[0][1], returned[:, width_a:]], axis=0)
    width = resid.shape[1]
    tok_rows = resid.shape[0]
    top_count = route_ids.shape[1]
    capacity = 3 * top_count * tok_rows // (2 * sp_ways)
    own_slots = slot_numbers(route_ids, sp_ways, capacity)
    term = jnp.dot(heads_out_a, proj_a, preferred_element_type=jnp.float32)
    term = term + jnp.dot(heads_out_b, proj_b, preferred_element_type=jnp.float32)
    mixed = resid.astype(jnp.float32) + lax.psum_scatter(
        lax.optimization_barrier(term.astype(jnp.bfloat16))
        .astype(jnp.float32)
        .astype(jnp.bfloat16),
        "tp",
        scatter_dimension=0,
        tiled=True,
    ).astype(jnp.float32)
    normed = rms_scaled(mixed, norm_gain).astype(jnp.bfloat16)
    lookup = jnp.arange(sp_ways * capacity, dtype=jnp.int32)[:, None]
    spread = jnp.zeros((sp_ways * capacity, tok_rows), jnp.float32)
    for which in range(top_count):
        spread = spread + (own_slots[:, which][None, :] == lookup).astype(jnp.float32)
    outgoing = jnp.dot(
        spread.astype(jnp.bfloat16), normed, preferred_element_type=jnp.float32
    ).astype(jnp.bfloat16)
    arrived = lax.all_to_all(
        outgoing.reshape(sp_ways, capacity, width), "sp", split_axis=0, concat_axis=0, tiled=True
    )
    piece = lax.all_gather(arrived.reshape(sp_ways * capacity, width), "tp", axis=0, tiled=True)
    gate = jnp.dot(piece, expert_gate[0], preferred_element_type=jnp.float32)
    upward = jnp.dot(piece, expert_up[0], preferred_element_type=jnp.float32)
    hidden = (jax.nn.silu(gate) * upward).astype(jnp.bfloat16)
    term = jnp.dot(hidden, expert_down[0], preferred_element_type=jnp.float32)
    summed = lax.psum_scatter(
        lax.optimization_barrier(term.astype(jnp.bfloat16))
        .astype(jnp.float32)
        .astype(jnp.bfloat16),
        "tp",
        scatter_dimension=0,
        tiled=True,
    )
    finished_rows = summed.reshape(sp_ways, capacity, width)
    back = lax.all_to_all(finished_rows, "sp", split_axis=0, concat_axis=0, tiled=True)
    picked = jnp.take(back.reshape(sp_ways * capacity, width), own_slots.reshape(-1), axis=0)
    picked = picked.reshape(tok_rows, top_count, width)
    output = mixed + jnp.sum(route_weights[:, :, None] * picked.astype(jnp.float32), axis=1)
    return output.astype(jnp.bfloat16)


def solution(mesh):
    placed = (
        P(("sp", "tp"), None),
        P("sp", "tp", None),
        P("sp", "tp", None),
        P("sp", "tp", None),
        P("sp", "tp", None),
        P("sp", "tp", None),
        P("sp", "tp", None),
        P("tp"),
        P("tp"),
        P(),
        P(),
        P("tp", None),
        P("tp", None),
        P(),
        P(("sp", "tp"), None),
        P(("sp", "tp"), None),
        P("sp", None, "tp"),
        P("sp", None, "tp"),
        P("sp", "tp", None),
    )
    return jax.shard_map(
        per_device, mesh=mesh, in_specs=placed, out_specs=P(("sp", "tp"), None), check_vma=False
    )
```

profile of v0, /device:TPU:0, one launch (start us, length us, event | category | flops | bytes accessed | tf_op | source)
XLA Modules:
  0.0 423.4 jit_solution(7599969802928675392)
XLA Ops:
  19.5 4.5 %collective-permute-done = bf16[256,384]{0,1:T(8,128)(2,1)} collective-permute-done((bf16[256,384]{0,1:T(8,128)(2,1)}, bf16[256,384]{0,1:T(8,128)(2,1)}, u32[]{:S(2)}, u32[]{:S(2)}) %collective-permute-start) | collective-permute-done | bytes 196640 | tf_op jit(solution)/shard_map/ppermute | solution.py:14
  25.3 16.1 %all_gather.17 = bf16[2048,2,64]{0,2,1:T(8,128)(2,1)} all-gather(bf16[512,2,64]{0,2,1:T(8,128)(2,1)} %param.32), channel_id=1, replica_groups=mesh['sp'=4,'tp'=8] {'sp'}, dimensions={0}, use_global_device_ids=true | all-gather | bytes 655360 | tf_op jit(solution)/shard_map/all_gather | solution.py:165
  41.4 10.7 %all_gather.18 = bf16[2048,2,64]{0,2,1:T(8,128)(2,1)} all-gather(bf16[512,2,64]{0,2,1:T(8,128)(2,1)} %param.33), channel_id=1, replica_groups=mesh['sp'=4,'tp'=8] {'sp'}, dimensions={0}, use_global_device_ids=true | all-gather | bytes 655360 | tf_op jit(solution)/shard_map/all_gather | solution.py:166
  53.4 17.1 %all-gather.6.cloned.1.call-done = bf16[2048,2,128]{0,2,1:T(8,128)(2,1)} async-done(((bf16[512,2,128]{0,2,1:T(8,128)(2,1)}), bf16[2048,2,128]{0,2,1:T(8,128)(2,1)}) %all-gather.6.cloned.1.call-update) | async-done | bytes 1048592 | tf_op jit(solution)/shard_map/all_gather | solution.py:164
  74.9 65.4 %while.72 = (s32[]{:T(128)}, f32[256,2,128]{0,2,1:T(8,128)S(1)}, f32[2,256]{1,0:T(2,128)S(1)}, f32[2,256]{1,0:T(2,128)}, f32[256,2,128]{0,2,1:T(8,128)}, /*index...) while((s32[]{:T(128)}, f32[256,2,128]{0,2,1:T(8,128)S(1)}, ...), condition=%wide.region_24.25_spmd.clone, body=%wide.region_13.24_spmd.clone.sunk | while | flops 311958272 | bytes 29590432 | solution.py:101
  75.5 15.7 %conditional.6 = ((f32[256,2,128]{0,2,1:T(8,128)S(1)}, f32[2,256]{1,0:T(2,128)S(1)}, f32[2,256]{1,0:T(2,128)}, f32[256,2,128]{0,2,1:T(8,128)}, f32[2,256]{1,0:T(...) conditional(s32[]{:T(128)} %convert_element_type.167, ...), branch_computations={%region_14.14_spmd, %region_15.23_spmd} | conditional | flops 311958272 | bytes 29588914 | solution.py:99
  91.8 15.8 %conditional.6 = ((f32[256,2,128]{0,2,1:T(8,128)S(1)}, f32[2,256]{1,0:T(2,128)S(1)}, f32[2,256]{1,0:T(2,128)}, f32[256,2,128]{0,2,1:T(8,128)}, f32[2,256]{1,0:T(...) conditional(s32[]{:T(128)} %convert_element_type.167, ...), branch_computations={%region_14.14_spmd, %region_15.23_spmd} | conditional | flops 311958272 | bytes 29588914 | solution.py:99
  108.2 15.7 %conditional.6 = ((f32[256,2,128]{0,2,1:T(8,128)S(1)}, f32[2,256]{1,0:T(2,128)S(1)}, f32[2,256]{1,0:T(2,128)}, f32[256,2,128]{0,2,1:T(8,128)}, f32[2,256]{1,0:T(...) conditional(s32[]{:T(128)} %convert_element_type.167, ...), branch_computations={%region_14.14_spmd, %region_15.23_spmd} | conditional | flops 311958272 | bytes 29588914 | solution.py:99
  124.5 15.7 %conditional.6 = ((f32[256,2,128]{0,2,1:T(8,128)S(1)}, f32[2,256]{1,0:T(2,128)S(1)}, f32[2,256]{1,0:T(2,128)}, f32[256,2,128]{0,2,1:T(8,128)}, f32[2,256]{1,0:T(...) conditional(s32[]{:T(128)} %convert_element_type.167, ...), branch_computations={%region_14.14_spmd, %region_15.23_spmd} | conditional | flops 311958272 | bytes 29588914 | solution.py:99
  145.4 19.4 %while.71 = (s32[]{:T(128)}, f32[256,2,128]{0,2,1:T(8,128)S(1)}, f32[2,256]{1,0:T(2,128)S(1)}, f32[2,256]{1,0:T(2,128)}, f32[256,2,128]{0,2,1:T(8,128)}, /*index...) while((s32[]{:T(128)}, f32[256,2,128]{0,2,1:T(8,128)S(1)}, ...), condition=%wide.region_11.12_spmd, body=%wide.region_0.11_spmd.sunk | while | flops 311958016 | bytes 29587348 | solution.py:101
  146.0 16.9 %conditional.5 = ((f32[256,2,128]{0,2,1:T(8,128)S(1)}, f32[2,256]{1,0:T(2,128)S(1)}, f32[2,256]{1,0:T(2,128)}, f32[256,2,128]{0,2,1:T(8,128)}, f32[2,256]{1,0:T(...) conditional(s32[]{:T(128)} %convert_element_type.166, ...), branch_computations={%region_1.0_spmd, %region_2.10_spmd} | conditional | flops 311958016 | bytes 29586862 | solution.py:99
  171.8 4.7 %collective-permute-done.2 = bf16[256,384]{0,1:T(8,128)(2,1)S(1)} collective-permute-done((bf16[256,384]{0,1:T(8,128)(2,1)S(1)}, bf16[256,384]{0,1:T(8,128)(2,1)S(1)}, u32[]{:S(2)}, u32[]{:S(2)}) %collective-permute-start.2) | collective-permute-done | bytes 196640 | tf_op jit(solution)/shard_map/ppermute | solution.py:14
  179.4 3.9 collective-permute-done.3
  187.2 36.5 %reduce-scatter.3.cloned.1.call-done = bf16[64,2048]{1,0:T(8,128)(2,1)} async-done(((bf16[512,2048]{1,0:T(8,128)(2,1)}), bf16[64,2048]{1,0:T(8,128)(2,1)}) %reduce-scatter.3.cloned.1.call-update) | async-done | bytes 262160 | tf_op jit(solution)/shard_map/reduce_scatter | solution.py:186
  226.3 12.3 %all_to_all.10 = bf16[4,48,2048]{2,1,0:T(8,128)(2,1)} all-to-all(bf16[4,48,2048]{2,1,0:T(8,128)(2,1)S(1)} %bitcast.127), channel_id=1, replica_groups=mesh['sp'=4,'tp'=8] {'sp'}, dimensions={0} | all-to-all | bytes 1572864 | tf_op jit(solution)/shard_map/all_to_all | solution.py:202
  238.8 63.9 %all-gather.8.cloned.1.call-done = bf16[1536,2048]{1,0:T(8,128)(2,1)} async-done(((bf16[192,2048]{1,0:T(8,128)(2,1)}), bf16[1536,2048]{1,0:T(8,128)(2,1)}) %all-gather.8.cloned.1.call-update) | async-done | bytes 6291472 | tf_op jit(solution)/shard_map/all_gather | solution.py:205
  302.7 8.2 %fusion.132 = f32[1536,768]{1,0:T(8,128)S(1)} fusion(bf16[1536,2048]{1,0:T(8,128)(2,1)} %all-gather.8.cloned.1.call-done, bf16[1,2048,768]{2,1,0:T(8,128)(2,1)} %param.43), kind=kOutput, calls=%fused_computation.172 | convolution fusion | flops 4831838208 | bytes 14155776 | tf_op jit(solution)/shard_map/dot_general | solution.py:206
  311.0 5.6 %multiply_convert_fusion = bf16[1536,768]{1,0:T(8,128)(2,1)S(1)} fusion(f32[1536,768]{1,0:T(8,128)S(1)} %fusion.132, bf16[1536,2048]{1,0:T(8,128)(2,1)S(1)} %copy-done.24, bf16[1,2048,768]{2,1,0:T(8,128)(2,1)S(1)} %copy-done.25), kind=kOutput, calls=%fused_computation.168 | convolution fusion | flops 4838916096 | bytes 16515072 | tf_op jit(solution)/shard_map/dot_general | solution.py:207
  316.6 7.1 %convolution_convert_fusion = bf16[1536,2048]{1,0:T(8,128)(2,1)} fusion(bf16[1536,768]{1,0:T(8,128)(2,1)S(1)} %multiply_convert_fusion, bf16[1,768,2048]{2,1,0:T(8,128)(2,1)S(1)} %copy-done), kind=kOutput, calls=%fused_computation.167 | convolution fusion | flops 4834983936 | bytes 11796480 | tf_op jit(solution)/shard_map/dot_general | solution.py:209
  323.7 68.5 %reduce-scatter.5.cloned.1.call-done = bf16[192,2048]{1,0:T(8,128)(2,1)} async-done(((bf16[1536,2048]{1,0:T(8,128)(2,1)}), bf16[192,2048]{1,0:T(8,128)(2,1)}) %reduce-scatter.5.cloned.1.call-update) | async-done | bytes 786448 | tf_op jit(solution)/shard_map/reduce_scatter | solution.py:210
  392.3 4.2 all-to-all-start.1
  396.9 8.8 %all-to-all-done.1 = bf16[4,48,2048]{2,1,0:T(8,128)(2,1)} async-done(((bf16[4,48,2048]{2,1,0:T(8,128)(2,1)}), bf16[4,48,2048]{2,1,0:T(8,128)(2,1)}, u32[]{:S(2)}, u32[]{:S(2)}) %all-to-all-start.1) | async-done | bytes 786464 | tf_op jit(solution)/shard_map/all_to_all | solution.py:219
  405.7 3.5 gather_fusion
  411.4 3.7 multiply_reduce_fusion
  (302 shorter events, 124.8 us)
Async XLA Ops:
  6.5 310.0 %copy-start = (bf16[1,768,2048]{2,1,0:T(8,128)(2,1)S(1)}, bf16[1,768,2048]{2,1,0:T(8,128)(2,1)}, u32[]{:S(2)}) copy-start(bf16[1,768,2048]{2,1,0:T(8,128)(2,1)} %param.45) | copy-start | bytes 9437188
  6.5 46.9 %all-gather.4.cloned.1.call-start = ((), (), s32[]{:S(2)}) async-start(), calls=%async_computation.4 | async-start | bytes 1310720 | tf_op jit(solution)/shard_map/all_gather | solution.py:163
  8.5 62.0 %all-gather.6.cloned.1.call-start = ((), (), s32[]{:S(2)}) async-start(), calls=%async_computation.5 | async-start | bytes 1310720 | tf_op jit(solution)/shard_map/all_gather | solution.py:164
  10.4 213.3 %reduce-scatter.3.cloned.1.call-start = ((), (), s32[]{:S(2)}) async-start(), calls=%async_computation.6 | async-start | bytes 2359296 | tf_op jit(solution)/shard_map/reduce_scatter | solution.py:186
  14.0 10.0 %collective-permute-start = (bf16[256,384]{0,1:T(8,128)(2,1)}, bf16[256,384]{0,1:T(8,128)(2,1)}, u32[]{:S(2)}, u32[]{:S(2)}) collective-permute-start(bf16[256,384]{0,1:T(8,128)(2,1)} %pad_maximum_fusion), channel_id=1, source_target_pairs={{0,8},{8,0},{16,24},{24,16},{1,9},{9,1},{17,25},{25,17},{2,10},{10... | collective-permute-start | bytes 589832 | tf_op jit(solution)/shard_map/ppermute | solution.py:14
  24.0 28.1 %collective-permute-start.1 = (bf16[256,384]{0,1:T(8,128)(2,1)}, bf16[256,384]{0,1:T(8,128)(2,1)S(1)}, u32[]{:S(2)}, u32[]{:S(2)}) collective-permute-start(bf16[256,384]{0,1:T(8,128)(2,1)} %collective-permute-done), channel_id=1, source_target_pairs={{0,16},{8,24},{16,0},{24,8},{1,17},{9,25},{17,1},{25,9},{2,18},{10... | collective-permute-start | bytes 589832 | tf_op jit(solution)/shard_map/ppermute | solution.py:14
  94.9 8.0 %copy-start.3 = (bf16[2048,2,128]{0,2,1:T(8,128)(2,1)S(1)}, bf16[2048,2,128]{0,2,1:T(8,128)(2,1)}, u32[]{:S(2)}) copy-start(bf16[2048,2,128]{0,2,1:T(8,128)(2,1)} %get-tuple-element.863) | copy-start | bytes 3145732 | tf_op jit(solution)/shard_map/while/body/eval_jaxpr/cond
  94.9 8.0 %copy-start.10 = (f32[256,2,128]{0,2,1:T(8,128)S(1)}, f32[256,2,128]{0,2,1:T(8,128)}, u32[]{:S(2)}) copy-start(f32[256,2,128]{0,2,1:T(8,128)} %get-tuple-element.865) | copy-start | bytes 786436 | tf_op jit(solution)/shard_map/while/body/eval_jaxpr/cond
  94.9 8.0 %copy-start.19 = (f32[256,2]{0,1:T(2,128)S(1)}, f32[256,2]{0,1:T(2,128)}, u32[]{:S(2)}) copy-start(f32[256,2]{0,1:T(2,128)} %get-tuple-element.1107) | copy-start | bytes 6148 | tf_op jit(solution)/shard_map/while/body/eval_jaxpr/cond
  111.2 8.0 %copy-start.3 = (bf16[2048,2,128]{0,2,1:T(8,128)(2,1)S(1)}, bf16[2048,2,128]{0,2,1:T(8,128)(2,1)}, u32[]{:S(2)}) copy-start(bf16[2048,2,128]{0,2,1:T(8,128)(2,1)} %get-tuple-element.863) | copy-start | bytes 3145732 | tf_op jit(solution)/shard_map/while/body/eval_jaxpr/cond
  111.2 8.0 %copy-start.10 = (f32[256,2,128]{0,2,1:T(8,128)S(1)}, f32[256,2,128]{0,2,1:T(8,128)}, u32[]{:S(2)}) copy-start(f32[256,2,128]{0,2,1:T(8,128)} %get-tuple-element.865) | copy-start | bytes 786436 | tf_op jit(solution)/shard_map/while/body/eval_jaxpr/cond
  111.2 8.0 %copy-start.19 = (f32[256,2]{0,1:T(2,128)S(1)}, f32[256,2]{0,1:T(2,128)}, u32[]{:S(2)}) copy-start(f32[256,2]{0,1:T(2,128)} %get-tuple-element.1107) | copy-start | bytes 6148 | tf_op jit(solution)/shard_map/while/body/eval_jaxpr/cond
  164.7 18.6 %copy-start.14 = (bf16[128,2048]{1,0:T(8,128)(2,1)S(1)}, bf16[128,2048]{1,0:T(8,128)(2,1)}, u32[]{:S(2)}) copy-start(bf16[128,2048]{1,0:T(8,128)(2,1)} %param.39) | copy-start | bytes 1572868
  166.1 18.0 %copy-start.13 = (bf16[256,2048]{1,0:T(8,128)(2,1)S(1)}, bf16[256,2048]{1,0:T(8,128)(2,1)}, u32[]{:S(2)}) copy-start(bf16[256,2048]{1,0:T(8,128)(2,1)} %param.38) | copy-start | bytes 3145732
  169.0 7.5 %collective-permute-start.2 = (bf16[256,384]{0,1:T(8,128)(2,1)S(1)}, bf16[256,384]{0,1:T(8,128)(2,1)S(1)}, u32[]{:S(2)}, u32[]{:S(2)}) collective-permute-start(bf16[256,384]{0,1:T(8,128)(2,1)S(1)} %pad_maximum_fusion.1), channel_id=1, source_target_pairs={{0,8},{8,0},{16,24},{24,16},{1,9},{9,1},{17,25},{25,17},{2,10},{10... | collective-permute-start | bytes 589832 | tf_op jit(solution)/shard_map/ppermute | solution.py:14
  176.5 6.9 %collective-permute-start.3 = (bf16[256,384]{0,1:T(8,128)(2,1)S(1)}, bf16[256,384]{0,1:T(8,128)(2,1)S(1)}, u32[]{:S(2)}, u32[]{:S(2)}) collective-permute-start(bf16[256,384]{0,1:T(8,128)(2,1)S(1)} %collective-permute-done.2), channel_id=1, source_target_pairs={{0,16},{8,24},{16,0},{24,8},{1,17},{9,25},{17,1},{25,9},{2,18},{10... | collective-permute-start | bytes 589832 | tf_op jit(solution)/shard_map/ppermute | solution.py:14
  184.1 39.6 %copy-start.12 = (bf16[64,2048]{1,0:T(8,128)(2,1)S(1)}, bf16[64,2048]{1,0:T(8,128)(2,1)}, u32[]{:S(2)}) copy-start(bf16[64,2048]{1,0:T(8,128)(2,1)} %param.27) | copy-start | bytes 786436
  184.1 40.8 %copy-start.22 = (f32[2048]{0:T(1024)S(1)}, f32[2048]{0:T(1024)}, u32[]{:S(2)}) copy-start(f32[2048]{0:T(1024)} %param.40) | copy-start | bytes 24580
  186.3 116.5 %all-gather.8.cloned.1.call-start = ((), (), s32[]{:S(2)}) async-start(), calls=%async_computation.7 | async-start | bytes 7077888 | tf_op jit(solution)/shard_map/all_gather | solution.py:205
  238.6 153.7 %reduce-scatter.5.cloned.1.call-start = ((), (), s32[]{:S(2)}) async-start(), calls=%async_computation.8 | async-start | bytes 7077888 | tf_op jit(solution)/shard_map/reduce_scatter | solution.py:210
  302.7 8.2 %copy-start.24 = (bf16[1536,2048]{1,0:T(8,128)(2,1)S(1)}, bf16[1536,2048]{1,0:T(8,128)(2,1)}, u32[]{:S(2)}) copy-start(bf16[1536,2048]{1,0:T(8,128)(2,1)} %all-gather.8.cloned.1.call-done) | copy-start | bytes 18874372
  302.7 8.2 %copy-start.25 = (bf16[1,2048,768]{2,1,0:T(8,128)(2,1)S(1)}, bf16[1,2048,768]{2,1,0:T(8,128)(2,1)}, u32[]{:S(2)}) copy-start(bf16[1,2048,768]{2,1,0:T(8,128)(2,1)} %param.44) | copy-start | bytes 9437188
  323.7 73.1 %copy-start.23 = (f32[64,2]{0,1:T(2,128)S(1)}, f32[64,2]{0,1:T(2,128)}, u32[]{:S(2)}) copy-start(f32[64,2]{0,1:T(2,128)} %param.42) | copy-start | bytes 1540
  392.3 13.5 %all-to-all-start.1 = ((bf16[4,48,2048]{2,1,0:T(8,128)(2,1)}), bf16[4,48,2048]{2,1,0:T(8,128)(2,1)}, u32[]{:S(2)}, u32[]{:S(2)}) async-start(bf16[4,48,2048]{2,1,0:T(8,128)(2,1)} %bitcast.128), calls=%async_computation.3 | async-start | bytes 1572864 | tf_op jit(solution)/shard_map/all_to_all | solution.py:219
  (36 other events, 182.1 us)
Sparse Core Ops, SparseCore 0:
  9.2 32.6 all-gather.3
  43.7 26.7 all-gather.5
  186.4 37.3 reduce-scatter.2
  238.7 63.9 all-gather.7
  323.8 68.3 reduce-scatter.4
where the time goes:
time: 425 us; the launch traced here: 423 us
  waiting for transfers between devices  208 us (49%)
  matrix products  78.7 us (19%)
  blocking collectives  39.1 us (9%)
  other arithmetic  36.5 us (9%)
  local copies, waits for them, and re-layouts  27.2 us (6%)
  starting transfers between devices  14.5 us (3%)
  between operations  13.5 us (3%)
  loops' own time  5.82 us (1%)
    reduce_scatter x2, waiting for transfers between devices, per_device(): lax.psum_scatter(lax.optimization_barrier(term.astype(jnp.bfloat16)).asty...  105 us
    all_gather x1, waiting for transfers between devices, per_device(): lax.all_gather(arrived.reshape(sp_ways * capacity, width), 'tp', axis=0,...  63.9 us
    dot_general x20, matrix products, map_update(): jnp.einsum('qhd,khd->hqk', query, keys, preferred_element_type=jnp.float32)  30.7 us
    dot_general x20, matrix products, map_update(): jnp.einsum('hqk,khv->qhv', weights.astype(jnp.bfloat16), values, preferre...  22.8 us
    all_gather x1, waiting for transfers between devices, per_device(): lax.all_gather(value_a, 'sp', axis=0, tiled=True)  17.1 us
    all_gather x1, blocking collectives, per_device(): lax.all_gather(key_b, 'sp', axis=0, tiled=True)  16.1 us
    ppermute x4, waiting for transfers between devices, partner(): lax.ppermute(value, axis, [(i, i ^ 1 << apart) for i in range(lax.axis_si...  13.2 us
    add x10, other arithmetic, map_update(): sums = sums * factor + jnp.sum(weights, axis=2)  12.9 us
  transfers between devices with their start and end apart: 10, of which 8 were waited for; matrix products, arithmetic and copies ran while one was open for 2% of the time, Pallas kernels for 0%

commit v1 on v0

--- a/solution.py
+++ b/solution.py
@@ -202,7 +202,11 @@
     arrived = lax.all_to_all(
         outgoing.reshape(sp_ways, capacity, width), "sp", split_axis=0, concat_axis=0, tiled=True
     )
-    piece = lax.all_gather(arrived.reshape(sp_ways * capacity, width), "tp", axis=0, tiled=True)
+    store_corner = lambda xs: jnp.concatenate(
+        lax.all_to_all(jnp.stack([xs for _ in range(lax.psum(1, "tp"))], axis=0), "tp", 0, 0),
+        axis=0,
+    )
+    piece = store_corner(arrived.reshape(sp_ways * capacity, width))
     gate = jnp.dot(piece, expert_gate[0], preferred_element_type=jnp.float32)
     upward = jnp.dot(piece, expert_up[0], preferred_element_type=jnp.float32)
     hidden = (jax.nn.silu(gate) * upward).astype(jnp.bfloat16)

time: 425 us -> 502 us (1.18)
  blocking collectives: 39.1 us -> 182 us
  waiting for transfers between devices: 208 us -> 143 us
    all_to_all x0 -> x1, blocking collectives: none -> 143 us  [per_device(): lax.all_to_all(jnp.stack([xs for _ in range(lax.psum(1, 'tp'))], axis=0),...]
    all_gather x1 -> x0, waiting for transfers between devices: 63.9 us -> none  [per_device(): lax.all_gather(arrived.reshape(sp_ways * capacity, width), 'tp', axis=0,...]
  transfers between devices with their start and end apart: 10 -> 9, of which waited for: 8 -> 7; matrix products, arithmetic and copies ran while one was open for 2% -> 2% of each run, Pallas kernels for 0% -> 0%
where the time goes in v1:
time: 502 us; the launch traced here: 500 us
  blocking collectives  182 us (36%)
  waiting for transfers between devices  143 us (28%)
  matrix products  76 us (15%)
  other arithmetic  36.5 us (7%)
  local copies, waits for them, and re-layouts  28.2 us (6%)
  starting transfers between devices  14.6 us (3%)
  between operations  13.5 us (3%)
  loops' own time  6.34 us (1%)
    all_to_all x1, blocking collectives, per_device(): lax.all_to_all(jnp.stack([xs for _ in range(lax.psum(1, 'tp'))], axis=0),...  143 us
    reduce_scatter x2, waiting for transfers between devices, per_device(): lax.psum_scatter(lax.optimization_barrier(term.astype(jnp.bfloat16)).asty...  104 us
    dot_general x20, matrix products, map_update(): jnp.einsum('qhd,khd->hqk', query, keys, preferred_element_type=jnp.float32)  30.9 us
    dot_general x20, matrix products, map_update(): jnp.einsum('hqk,khv->qhv', weights.astype(jnp.bfloat16), values, preferre...  23 us
    all_gather x1, waiting for transfers between devices, per_device(): lax.all_gather(value_a, 'sp', axis=0, tiled=True)  17 us
    all_gather x1, blocking collectives, per_device(): lax.all_gather(key_b, 'sp', axis=0, tiled=True)  16.2 us
    ppermute x4, waiting for transfers between devices, partner(): lax.ppermute(value, axis, [(i, i ^ 1 << apart) for i in range(lax.axis_si...  13.1 us
    add x10, other arithmetic, map_update(): sums = sums * factor + jnp.sum(weights, axis=2)  12.9 us
  transfers between devices with their start and end apart: 9, of which 7 were waited for; matrix products, arithmetic and copies ran while one was open for 2% of the time, Pallas kernels for 0%

profile of v1, /device:TPU:0, one launch (start us, length us, event | category | flops | bytes accessed | tf_op | source)
XLA Modules:
  0.0 500.0 jit_solution(13080105872777136164)
XLA Ops:
  19.5 4.5 collective-permute-done
  25.3 16.2 %all_gather.14 = bf16[2048,2,64]{0,2,1:T(8,128)(2,1)} all-gather(bf16[512,2,64]{0,2,1:T(8,128)(2,1)} %param.32), channel_id=1, replica_groups=mesh['sp'=4,'tp'=8] {'sp'}, dimensions={0}, use_global_device_ids=true | all-gather | bytes 655360 | tf_op jit(solution)/shard_map/all_gather | solution.py:165
  41.4 10.7 %all_gather.15 = bf16[2048,2,64]{0,2,1:T(8,128)(2,1)} all-gather(bf16[512,2,64]{0,2,1:T(8,128)(2,1)} %param.33), channel_id=1, replica_groups=mesh['sp'=4,'tp'=8] {'sp'}, dimensions={0}, use_global_device_ids=true | all-gather | bytes 655360 | tf_op jit(solution)/shard_map/all_gather | solution.py:166
  53.4 17.0 %all-gather.5.cloned.1.call-done = bf16[2048,2,128]{0,2,1:T(8,128)(2,1)} async-done(((bf16[512,2,128]{0,2,1:T(8,128)(2,1)}), bf16[2048,2,128]{0,2,1:T(8,128)(2,1)}) %all-gather.5.cloned.1.call-update) | async-done | bytes 1048592 | tf_op jit(solution)/shard_map/all_gather | solution.py:164
  74.9 65.9 %while.72 = (s32[]{:T(128)}, f32[256,2,128]{0,2,1:T(8,128)S(1)}, f32[2,256]{1,0:T(2,128)S(1)}, f32[2,256]{1,0:T(2,128)}, f32[256,2,128]{0,2,1:T(8,128)}, /*index...) while((s32[]{:T(128)}, f32[256,2,128]{0,2,1:T(8,128)S(1)}, ...), condition=%wide.region_24.25_spmd.clone, body=%wide.region_13.24_spmd.clone.sunk | while | flops 311958272 | bytes 29590432 | solution.py:101
  75.6 15.8 %conditional.6 = ((f32[256,2,128]{0,2,1:T(8,128)S(1)}, f32[2,256]{1,0:T(2,128)S(1)}, f32[2,256]{1,0:T(2,128)}, f32[256,2,128]{0,2,1:T(8,128)}, f32[2,256]{1,0:T(...) conditional(s32[]{:T(128)} %convert_element_type.167, ...), branch_computations={%region_14.14_spmd, %region_15.23_spmd} | conditional | flops 311958272 | bytes 29588914 | solution.py:99
  92.0 15.8 %conditional.6 = ((f32[256,2,128]{0,2,1:T(8,128)S(1)}, f32[2,256]{1,0:T(2,128)S(1)}, f32[2,256]{1,0:T(2,128)}, f32[256,2,128]{0,2,1:T(8,128)}, f32[2,256]{1,0:T(...) conditional(s32[]{:T(128)} %convert_element_type.167, ...), branch_computations={%region_14.14_spmd, %region_15.23_spmd} | conditional | flops 311958272 | bytes 29588914 | solution.py:99
  108.5 15.8 %conditional.6 = ((f32[256,2,128]{0,2,1:T(8,128)S(1)}, f32[2,256]{1,0:T(2,128)S(1)}, f32[2,256]{1,0:T(2,128)}, f32[256,2,128]{0,2,1:T(8,128)}, f32[2,256]{1,0:T(...) conditional(s32[]{:T(128)} %convert_element_type.167, ...), branch_computations={%region_14.14_spmd, %region_15.23_spmd} | conditional | flops 311958272 | bytes 29588914 | solution.py:99
  125.0 15.8 %conditional.6 = ((f32[256,2,128]{0,2,1:T(8,128)S(1)}, f32[2,256]{1,0:T(2,128)S(1)}, f32[2,256]{1,0:T(2,128)}, f32[256,2,128]{0,2,1:T(8,128)}, f32[2,256]{1,0:T(...) conditional(s32[]{:T(128)} %convert_element_type.167, ...), branch_computations={%region_14.14_spmd, %region_15.23_spmd} | conditional | flops 311958272 | bytes 29588914 | solution.py:99
  145.9 19.7 %while.71 = (s32[]{:T(128)}, f32[256,2,128]{0,2,1:T(8,128)S(1)}, f32[2,256]{1,0:T(2,128)S(1)}, f32[2,256]{1,0:T(2,128)}, f32[256,2,128]{0,2,1:T(8,128)}, /*index...) while((s32[]{:T(128)}, f32[256,2,128]{0,2,1:T(8,128)S(1)}, ...), condition=%wide.region_11.12_spmd, body=%wide.region_0.11_spmd.sunk | while | flops 311958016 | bytes 29587348 | solution.py:101
  146.6 17.0 %conditional.5 = ((f32[256,2,128]{0,2,1:T(8,128)S(1)}, f32[2,256]{1,0:T(2,128)S(1)}, f32[2,256]{1,0:T(2,128)}, f32[256,2,128]{0,2,1:T(8,128)}, f32[2,256]{1,0:T(...) conditional(s32[]{:T(128)} %convert_element_type.166, ...), branch_computations={%region_1.0_spmd, %region_2.10_spmd} | conditional | flops 311958016 | bytes 29586862 | solution.py:99
  172.7 4.7 collective-permute-done.2
  180.5 3.9 collective-permute-done.3
  188.3 36.7 %reduce-scatter.3.cloned.1.call-done = bf16[64,2048]{1,0:T(8,128)(2,1)} async-done(((bf16[512,2048]{1,0:T(8,128)(2,1)}), bf16[64,2048]{1,0:T(8,128)(2,1)}) %reduce-scatter.3.cloned.1.call-update) | async-done | bytes 262160 | tf_op jit(solution)/shard_map/reduce_scatter | solution.py:186
  227.6 12.0 %all_to_all.15 = bf16[4,48,2048]{2,1,0:T(8,128)(2,1)S(1)} all-to-all(bf16[4,48,2048]{2,1,0:T(8,128)(2,1)S(1)} %bitcast.130), channel_id=1, replica_groups=mesh['sp'=4,'tp'=8] {'sp'}, dimensions={0} | all-to-all | bytes 1572864 | tf_op jit(solution)/shard_map/all_to_all | solution.py:202
  240.3 143.4 %all_to_all.16 = bf16[8,192,2048]{2,1,0:T(8,128)(2,1)S(1)} all-to-all(bf16[8,192,2048]{2,1,0:T(8,128)(2,1)S(1)} %stack.3), channel_id=1, replica_groups=mesh['sp'=4,'tp'=8] {'tp'}, dimensions={0} | all-to-all | bytes 12582912 | tf_op jit(solution)/shard_map/all_to_all | solution.py:206
  383.7 5.2 %fusion.132 = f32[1536,768]{1,0:T(8,128)S(1)} fusion(bf16[1536,2048]{1,0:T(8,128)(2,1)S(1)} %bitcast.127, bf16[1,2048,768]{2,1,0:T(8,128)(2,1)S(1)} %copy-done.24), kind=kOutput, calls=%fused_computation.172 | convolution fusion | flops 4831838208 | bytes 14155776 | tf_op jit(solution)/shard_map/dot_general | solution.py:210
  388.9 5.6 %multiply_convert_fusion = bf16[1536,768]{1,0:T(8,128)(2,1)S(1)} fusion(f32[1536,768]{1,0:T(8,128)S(1)} %fusion.132, bf16[1536,2048]{1,0:T(8,128)(2,1)S(1)} %bitcast.128, bf16[1,2048,768]{2,1,0:T(8,128)(2,1)S(1)} %copy-done.25), kind=kOutput, calls=%fused_computation.168 | convolution fusion | flops 4838916096 | bytes 16515072 | tf_op jit(solution)/shard_map/dot_general | solution.py:211
  394.6 7.1 %convolution_convert_fusion = bf16[1536,2048]{1,0:T(8,128)(2,1)} fusion(bf16[1536,768]{1,0:T(8,128)(2,1)S(1)} %multiply_convert_fusion, bf16[1,768,2048]{2,1,0:T(8,128)(2,1)S(1)} %copy-done), kind=kOutput, calls=%fused_computation.167 | convolution fusion | flops 4834983936 | bytes 11796480 | tf_op jit(solution)/shard_map/dot_general | solution.py:213
  401.7 67.3 %reduce-scatter.5.cloned.1.call-done = bf16[192,2048]{1,0:T(8,128)(2,1)} async-done(((bf16[1536,2048]{1,0:T(8,128)(2,1)}), bf16[192,2048]{1,0:T(8,128)(2,1)}) %reduce-scatter.5.cloned.1.call-update) | async-done | bytes 786448 | tf_op jit(solution)/shard_map/reduce_scatter | solution.py:214
  469.0 4.4 all-to-all-start.2
  473.9 8.6 %all-to-all-done.2 = bf16[4,48,2048]{2,1,0:T(8,128)(2,1)} async-done(((bf16[4,48,2048]{2,1,0:T(8,128)(2,1)}), bf16[4,48,2048]{2,1,0:T(8,128)(2,1)}, u32[]{:S(2)}, u32[]{:S(2)}) %all-to-all-start.2) | async-done | bytes 786464 | tf_op jit(solution)/shard_map/all_to_all | solution.py:223
  482.4 3.5 gather_fusion
  488.1 3.7 multiply_reduce_fusion
  (301 shorter events, 125.9 us)
Async XLA Ops:
  6.5 388.0 %copy-start = (bf16[1,768,2048]{2,1,0:T(8,128)(2,1)S(1)}, bf16[1,768,2048]{2,1,0:T(8,128)(2,1)}, u32[]{:S(2)}) copy-start(bf16[1,768,2048]{2,1,0:T(8,128)(2,1)} %param.45) | copy-start | bytes 9437188
  6.5 46.9 %all-gather.3.cloned.1.call-start = ((), (), s32[]{:S(2)}) async-start(), calls=%async_computation.5 | async-start | bytes 1310720 | tf_op jit(solution)/shard_map/all_gather | solution.py:163
  8.5 61.9 %all-gather.5.cloned.1.call-start = ((), (), s32[]{:S(2)}) async-start(), calls=%async_computation.6 | async-start | bytes 1310720 | tf_op jit(solution)/shard_map/all_gather | solution.py:164
  10.4 214.6 %reduce-scatter.3.cloned.1.call-start = ((), (), s32[]{:S(2)}) async-start(), calls=%async_computation.7 | async-start | bytes 2359296 | tf_op jit(solution)/shard_map/reduce_scatter | solution.py:186
  13.9 10.0 %collective-permute-start = (bf16[256,384]{0,1:T(8,128)(2,1)}, bf16[256,384]{0,1:T(8,128)(2,1)}, u32[]{:S(2)}, u32[]{:S(2)}) collective-permute-start(bf16[256,384]{0,1:T(8,128)(2,1)} %pad_maximum_fusion), channel_id=1, source_target_pairs={{0,8},{8,0},{16,24},{24,16},{1,9},{9,1},{17,25},{25,17},{2,10},{10... | collective-permute-start | bytes 589832 | tf_op jit(solution)/shard_map/ppermute | solution.py:14
  24.0 28.1 %collective-permute-start.1 = (bf16[256,384]{0,1:T(8,128)(2,1)}, bf16[256,384]{0,1:T(8,128)(2,1)S(1)}, u32[]{:S(2)}, u32[]{:S(2)}) collective-permute-start(bf16[256,384]{0,1:T(8,128)(2,1)} %collective-permute-done), channel_id=1, source_target_pairs={{0,16},{8,24},{16,0},{24,8},{1,17},{9,25},{17,1},{25,9},{2,18},{10... | collective-permute-start | bytes 589832 | tf_op jit(solution)/shard_map/ppermute | solution.py:14
  78.6 8.0 %copy-start.10 = (f32[256,2,128]{0,2,1:T(8,128)S(1)}, f32[256,2,128]{0,2,1:T(8,128)}, u32[]{:S(2)}) copy-start(f32[256,2,128]{0,2,1:T(8,128)} %get-tuple-element.865) | copy-start | bytes 786436 | tf_op jit(solution)/shard_map/while/body/eval_jaxpr/cond
  95.1 8.0 %copy-start.3 = (bf16[2048,2,128]{0,2,1:T(8,128)(2,1)S(1)}, bf16[2048,2,128]{0,2,1:T(8,128)(2,1)}, u32[]{:S(2)}) copy-start(bf16[2048,2,128]{0,2,1:T(8,128)(2,1)} %get-tuple-element.863) | copy-start | bytes 3145732 | tf_op jit(solution)/shard_map/while/body/eval_jaxpr/cond
  95.1 8.0 %copy-start.10 = (f32[256,2,128]{0,2,1:T(8,128)S(1)}, f32[256,2,128]{0,2,1:T(8,128)}, u32[]{:S(2)}) copy-start(f32[256,2,128]{0,2,1:T(8,128)} %get-tuple-element.865) | copy-start | bytes 786436 | tf_op jit(solution)/shard_map/while/body/eval_jaxpr/cond
  111.6 8.0 %copy-start.3 = (bf16[2048,2,128]{0,2,1:T(8,128)(2,1)S(1)}, bf16[2048,2,128]{0,2,1:T(8,128)(2,1)}, u32[]{:S(2)}) copy-start(bf16[2048,2,128]{0,2,1:T(8,128)(2,1)} %get-tuple-element.863) | copy-start | bytes 3145732 | tf_op jit(solution)/shard_map/while/body/eval_jaxpr/cond
  111.6 8.0 %copy-start.10 = (f32[256,2,128]{0,2,1:T(8,128)S(1)}, f32[256,2,128]{0,2,1:T(8,128)}, u32[]{:S(2)}) copy-start(f32[256,2,128]{0,2,1:T(8,128)} %get-tuple-element.865) | copy-start | bytes 786436 | tf_op jit(solution)/shard_map/while/body/eval_jaxpr/cond
  128.0 8.0 %copy-start.3 = (bf16[2048,2,128]{0,2,1:T(8,128)(2,1)S(1)}, bf16[2048,2,128]{0,2,1:T(8,128)(2,1)}, u32[]{:S(2)}) copy-start(bf16[2048,2,128]{0,2,1:T(8,128)(2,1)} %get-tuple-element.863) | copy-start | bytes 3145732 | tf_op jit(solution)/shard_map/while/body/eval_jaxpr/cond
  128.1 8.0 %copy-start.10 = (f32[256,2,128]{0,2,1:T(8,128)S(1)}, f32[256,2,128]{0,2,1:T(8,128)}, u32[]{:S(2)}) copy-start(f32[256,2,128]{0,2,1:T(8,128)} %get-tuple-element.865) | copy-start | bytes 786436 | tf_op jit(solution)/shard_map/while/body/eval_jaxpr/cond
  150.9 8.0 %copy-start.7 = (f32[256,2,128]{0,2,1:T(8,128)S(1)}, f32[256,2,128]{0,2,1:T(8,128)}, u32[]{:S(2)}) copy-start(f32[256,2,128]{0,2,1:T(8,128)} %get-tuple-element.811) | copy-start | bytes 786436 | tf_op jit(solution)/shard_map/while/body/eval_jaxpr/cond
  165.6 18.8 %copy-start.14 = (bf16[128,2048]{1,0:T(8,128)(2,1)S(1)}, bf16[128,2048]{1,0:T(8,128)(2,1)}, u32[]{:S(2)}) copy-start(bf16[128,2048]{1,0:T(8,128)(2,1)} %param.39) | copy-start | bytes 1572868
  167.0 18.2 %copy-start.13 = (bf16[256,2048]{1,0:T(8,128)(2,1)S(1)}, bf16[256,2048]{1,0:T(8,128)(2,1)}, u32[]{:S(2)}) copy-start(bf16[256,2048]{1,0:T(8,128)(2,1)} %param.38) | copy-start | bytes 3145732
  169.9 7.5 %collective-permute-start.2 = (bf16[256,384]{0,1:T(8,128)(2,1)S(1)}, bf16[256,384]{0,1:T(8,128)(2,1)S(1)}, u32[]{:S(2)}, u32[]{:S(2)}) collective-permute-start(bf16[256,384]{0,1:T(8,128)(2,1)S(1)} %pad_maximum_fusion.1), channel_id=1, source_target_pairs={{0,8},{8,0},{16,24},{24,16},{1,9},{9,1},{17,25},{25,17},{2,10},{10... | collective-permute-start | bytes 589832 | tf_op jit(solution)/shard_map/ppermute | solution.py:14
  177.4 7.0 %collective-permute-start.3 = (bf16[256,384]{0,1:T(8,128)(2,1)S(1)}, bf16[256,384]{0,1:T(8,128)(2,1)S(1)}, u32[]{:S(2)}, u32[]{:S(2)}) collective-permute-start(bf16[256,384]{0,1:T(8,128)(2,1)S(1)} %collective-permute-done.2), channel_id=1, source_target_pairs={{0,16},{8,24},{16,0},{24,8},{1,17},{9,25},{17,1},{25,9},{2,18},{10... | collective-permute-start | bytes 589832 | tf_op jit(solution)/shard_map/ppermute | solution.py:14
  185.2 39.9 %copy-start.12 = (bf16[64,2048]{1,0:T(8,128)(2,1)S(1)}, bf16[64,2048]{1,0:T(8,128)(2,1)}, u32[]{:S(2)}) copy-start(bf16[64,2048]{1,0:T(8,128)(2,1)} %param.27) | copy-start | bytes 786436
  185.2 41.0 %copy-start.22 = (f32[2048]{0:T(1024)S(1)}, f32[2048]{0:T(1024)}, u32[]{:S(2)}) copy-start(f32[2048]{0:T(1024)} %param.40) | copy-start | bytes 24580
  187.3 281.7 %reduce-scatter.5.cloned.1.call-start = ((), (), s32[]{:S(2)}) async-start(), calls=%async_computation.8 | async-start | bytes 7077888 | tf_op jit(solution)/shard_map/reduce_scatter | solution.py:214
  240.3 143.4 %copy-start.24 = (bf16[1,2048,768]{2,1,0:T(8,128)(2,1)S(1)}, bf16[1,2048,768]{2,1,0:T(8,128)(2,1)}, u32[]{:S(2)}) copy-start(bf16[1,2048,768]{2,1,0:T(8,128)(2,1)} %param.43) | copy-start | bytes 9437188
  401.6 72.1 %copy-start.23 = (f32[64,2]{0,1:T(2,128)S(1)}, f32[64,2]{0,1:T(2,128)}, u32[]{:S(2)}) copy-start(f32[64,2]{0,1:T(2,128)} %param.42) | copy-start | bytes 1540
  469.0 13.5 %all-to-all-start.2 = ((bf16[4,48,2048]{2,1,0:T(8,128)(2,1)}), bf16[4,48,2048]{2,1,0:T(8,128)(2,1)}, u32[]{:S(2)}, u32[]{:S(2)}) async-start(bf16[4,48,2048]{2,1,0:T(8,128)(2,1)} %bitcast.131), calls=%async_computation.4 | async-start | bytes 1572864 | tf_op jit(solution)/shard_map/all_to_all | solution.py:223
  (35 other events, 171.8 us)
Sparse Core Ops, SparseCore 0:
  9.2 32.6 all-gather.2
  43.7 26.7 all-gather.4
  187.4 37.5 reduce-scatter.2
  401.8 67.1 reduce-scatter.4
